TPU v7x, 128 devices: a whole 4x4x4 slice. The times are simulated.
128 devices in a mesh: sp: 16 (over z, y), tp: 8 (over x, core).
Axes of the slice: x: 4, y: 4, z: 4, core: 2. Of those that a mesh axis runs over, the one named last changes fastest.
Arguments:
- queries: bfloat16 [12288, 2048], P('sp', 'tp'), may hold values from -11 to 11
- key_rows: bfloat16 [12288, 2048], P('sp', 'tp'), may hold values from -4.5 to 4.5
- value_rows: bfloat16 [12288, 2048], P('sp', 'tp'), may hold values from -6 to 6
- log_forget: float32 [12288, 32], P('sp', 'tp'), may hold values from -1477.56 to 0, as said below
- stream_in: bfloat16 [12288, 2048], P('sp'), may hold values from -6 to 6
- out_weight: bfloat16 [2048, 2048], P('tp'), may hold values from -0.52734375 to 0.52734375
- mix_gain: float32 [2048], replicated, may hold values from 0.1 to 1.9
- mix_bias: float32 [2048], replicated, may hold values from -3 to 3
- gate_weight: bfloat16 [2048, 5632], P('sp', 'tp'), may hold values from -0.125 to 0.125
- up_weight: bfloat16 [2048, 5632], P('sp', 'tp'), may hold values from -0.125 to 0.125
- down_weight: bfloat16 [5632, 2048], P('tp', 'sp'), may hold values from -0.15917969 to 0.15917969
- ffn_gain: float32 [2048], replicated, may hold values from 0.1 to 1.9
- ffn_bias: float32 [2048], replicated, may hold values from -3 to 3
Outputs:
- layer_out: bfloat16 [12288, 2048], P(('sp', 'tp'))
Inputs may be any that keep to these rules, and one draw needn't show every extreme that they name: `log_forget`: each column never rises along the positions.
All inputs are finite; a program needn't handle non-finite values.
Results may differ from a plain program's by a relative error of at most 0.015.
Values may be sent and summed in bfloat16 or wider, within the bound.
A program may use at most 128 MiB of HBM per device.

v0:
```python
import jax
import jax.numpy as jnp
from jax import lax
from jax.sharding import PartitionSpec as P

ALPHA = 8.0**0.25
EPSILON = 1e-05


def laid_out(pieces, dim):
    lengths = list(pieces.shape[1:])
    lengths[dim] *= pieces.shape[0]
    return jnp.moveaxis(pieces, 0, dim).reshape(lengths)


def from_everyone(value, axis):
    copies = jnp.broadcast_to(value, (lax.axis_size(axis), *value.shape))
    return lax.all_to_all(copies, axis, split_axis=0, concat_axis=0, tiled=True)


def gathered_copies(value, axis, dim):
    return laid_out(from_everyone(value, axis), dim)


def in_one_piece(arrays, axis, dim, along):
    ends, at = ([], 0)
    for a in arrays[:-1]:
        at += a.shape[along]
        ends.append(at)
    both = jnp.concatenate(arrays, axis=along)
    return tuple(jnp.split(lax.all_gather(both, axis, axis=dim, tiled=True), ends, axis=along))


def in_blocks(value, dim, count):
    before, after = (value.shape[:dim], value.shape[dim + 1 :])
    return jnp.moveaxis(value.reshape(*before, count, -1, *after), dim, 0)


def sum_at_owner(value, axis, dim):
    pieces = in_blocks(value, dim, lax.axis_size(axis))
    arrived = lax.all_to_all(pieces, axis, split_axis=0, concat_axis=0, tiled=True)
    return arrived.astype(jnp.float32).sum(axis=0)


def layer_norm(matrix, norm_gain, norm_shift):
    centred = matrix - jnp.mean(matrix, axis=-1, keepdims=True)
    spread = jnp.mean(centred * centred, axis=-1, keepdims=True)
    return centred * lax.rsqrt(spread + EPSILON) * norm_gain + norm_shift


def attend(queries, key_rows, value_rows, log_forget):
    length, row_width = queries.shape
    head_count = log_forget.shape[1]
    head_dim = row_width // head_count
    score_scale = head_dim ** (-0.5)
    first_pos = lax.axis_index("sp") * length
    last_pos = first_pos + length
    query_heads = queries.reshape(length, head_count, head_dim)
    query_gates = log_forget.T
    query_pos = first_pos + jnp.arange(length, dtype=jnp.int32)
    gates_all = gathered_copies(log_forget, "sp", 0)
    initial = (
        jnp.full((head_count, length), -1e30, jnp.float32),
        jnp.zeros((head_count, length), jnp.float32),
        jnp.zeros((length, head_count, head_dim), jnp.float32),
    )
    running = initial
    key_piece, value_piece = in_one_piece((key_rows, value_rows), "sp", 0, 1)
    piece_len = key_piece.shape[0]
    shards = piece_len // length
    group_size = max(
        [
            count_try
            for count_try in range(1, shards + 1)
            if shards % count_try == 0 and count_try * length <= max(length, 512)
        ]
    )
    block_len = group_size * length
    blocks = piece_len // block_len
    key_blocks = key_piece.reshape(blocks, block_len, head_count, head_dim)
    value_blocks = value_piece.reshape(blocks, block_len, head_count, head_dim)
    gate_blocks = gates_all.reshape(blocks, block_len, head_count)
    block_starts = block_len * jnp.arange(blocks, dtype=jnp.int32)

    def one_block(running_state, packed):
        key_block, value_block, gate_block, block_start = packed

        def compute(state_in):
            highest, totals, weighted = state_in
            scores = (
                jnp.einsum(
                    "qhd,khd->hqk", query_heads, key_block, preferred_element_type=jnp.float32
                )
                * score_scale
            )
            scores = scores + query_gates[:, :, None] - gate_block.T[:, None, :]
            key_pos = block_start + jnp.arange(block_len, dtype=jnp.int32)
            allowed = (key_pos[None, :] <= query_pos[:, None])[None]
            masked = jnp.where(allowed, scores, -1e30)
            new_high = jnp.maximum(highest, jnp.max(masked, axis=2))
            weights = jnp.where(allowed, jnp.exp(masked - new_high[:, :, None]), 0.0)
            factor = jnp.exp(highest - new_high)
            totals = totals * factor + jnp.sum(weights, axis=2)
            weighted = weighted * factor.T[:, :, None] + jnp.einsum(
                "hqk,khd->qhd",
                weights.astype(jnp.bfloat16),
                value_block,
                preferred_element_type=jnp.float32,
            )
            return (new_high, totals, weighted)

        def keep_state(state_in):
            return state_in

        return (lax.cond(block_start < last_pos, compute, keep_state, running_state), None)

    running, unused = lax.scan(
        one_block, running, (key_blocks, value_blocks, gate_blocks, block_starts)
    )
    highest, totals, weighted = running
    return (weighted / totals.T[:, :, None]).reshape(length, row_width).astype(jnp.bfloat16)


def body(
    queries,
    key_rows,
    value_rows,
    log_forget,
    stream_in,
    out_weight,
    mix_gain,
    mix_bias,
    gate_weight,
    up_weight,
    down_weight,
    ffn_gain,
    ffn_bias,
):
    attended = attend(queries, key_rows, value_rows, log_forget)
    length = attended.shape[0]
    own_rows = length // lax.axis_size("tp")
    offset = lax.axis_index("tp") * own_rows
    summed = sum_at_owner(
        jnp.dot(attended, out_weight, preferred_element_type=jnp.float32).astype(jnp.bfloat16),
        "tp",
        0,
    )
    mix_out = lax.optimization_barrier(summed.astype(jnp.bfloat16)).astype(jnp.float32)
    stream_own = lax.dynamic_slice_in_dim(stream_in, offset, own_rows, 0)
    normed = layer_norm(
        ALPHA * stream_own.astype(jnp.float32) + mix_out, mix_gain, mix_bias
    ).astype(jnp.bfloat16)
    gathered = lax.all_gather(normed, "tp", axis=0, tiled=True)
    pieces = in_one_piece((gate_weight, up_weight), "sp", 0, 1)
    gate_part = jnp.dot(gathered, pieces[0], preferred_element_type=jnp.float32)
    up_part = jnp.dot(gathered, pieces[1], preferred_element_type=jnp.float32)
    hidden = (jax.nn.silu(gate_part) * up_part).astype(jnp.bfloat16)
    partial_terms = jnp.dot(
        hidden,
        lax.all_gather(down_weight, "sp", axis=1, tiled=True),
        preferred_element_type=jnp.float32,
    )
    lowered = lax.psum_scatter(
        partial_terms.astype(jnp.bfloat16), "tp", scatter_dimension=0, tiled=True
    ).astype(jnp.float32)
    lowered = lax.optimization_barrier(lowered.astype(jnp.bfloat16)).astype(jnp.float32)
    result = layer_norm(ALPHA * normed.astype(jnp.float32) + lowered, ffn_gain, ffn_bias)
    return result.astype(jnp.bfloat16)


def solution(mesh):
    placed = (
        P("sp", "tp"),
        P("sp", "tp"),
        P("sp", "tp"),
        P("sp", "tp"),
        P("sp", None),
        P("tp", None),
        P(),
        P(),
        P("sp", "tp"),
        P("sp", "tp"),
        P("tp", "sp"),
        P(),
        P(),
    )
    return jax.shard_map(
        body, mesh=mesh, in_specs=placed, out_specs=P(("sp", "tp"), None), check_vma=False
    )
```

profile of v0, /device:TPU:0, one launch (start us, length us, event | category | flops | bytes accessed | tf_op | source)
XLA Modules:
  0.0 604.3 jit_solution(4880820120093457124)
XLA Ops:
  6.5 2.2 pad_maximum_fusion
  8.7 0.0 all-gather.5.cloned.1.call-update
  8.8 0.0 all-gather.9.cloned.1.call-start
  8.8 1.8 pad_maximum_fusion.1
  10.6 0.0 all-gather.9.cloned.1.call-update
  10.6 1.4 broadcast_in_dim.56
  12.0 8.2 %all-to-all-start = ((f32[16,768,4]{1,2,0:T(4,128)}), f32[16,768,4]{1,2,0:T(4,128)S(1)}, u32[]{:S(2)}, u32[]{:S(2)}) async-start(f32[16,768,4]{1,2,0:T(4,128)} %broadcast_in_dim.56), calls=%async_computation | async-start | bytes 393216 | tf_op jit(solution)/shard_map/all_to_all | solution.py:18
  20.2 1.2 copy.18
  21.4 80.5 %all-gather.5.cloned.1.call-done = bf16[12288,512]{1,0:T(8,128)(2,1)} async-done(((bf16[768,512]{1,0:T(8,128)(2,1)}), bf16[12288,512]{1,0:T(8,128)(2,1)}) %all-gather.5.cloned.1.call-update) | async-done | bytes 12582928 | tf_op jit(solution)/shard_map/all_gather | solution.py:31
  101.9 10.1 %fusion.36 = (bf16[12288,256]{1,0:T(8,128)(2,1)}, bf16[12288,256]{1,0:T(8,128)(2,1)}) fusion(bf16[12288,512]{1,0:T(8,128)(2,1)} %all-gather.5.cloned.1.call-done), kind=kLoop, calls=%fused_computation.51 | loop fusion | bytes 25165824 | tf_op jit(solution)/shard_map/split | solution.py:31
  112.0 18.8 %reshape.82 = bf16[16,768,4,64]{3,2,1,0:T(4,128)(2,1)} reshape(bf16[12288,256]{1,0:T(8,128)(2,1)} %get-tuple-element.249) | data formatting | bytes 12582912 | tf_op jit(solution)/shard_map/reshape | solution.py:80
  130.8 18.1 %copy.20 = bf16[16,768,4,64]{1,3,2,0:T(8,128)(2,1)} copy(bf16[16,768,4,64]{3,2,1,0:T(4,128)(2,1)} %reshape.82) | data formatting | bytes 12582912
  148.9 18.8 %reshape.83 = bf16[16,768,4,64]{3,2,1,0:T(4,128)(2,1)} reshape(bf16[12288,256]{1,0:T(8,128)(2,1)} %get-tuple-element.248) | data formatting | bytes 12582912 | tf_op jit(solution)/shard_map/reshape | solution.py:81
  167.6 18.1 %copy.21 = bf16[16,768,4,64]{1,3,2,0:T(8,128)(2,1)} copy(bf16[16,768,4,64]{3,2,1,0:T(4,128)(2,1)} %reshape.83) | data formatting | bytes 12582912
  185.7 0.0 all-to-all-done
  185.7 0.1 broadcast_in_dim.55
  185.8 33.5 %while.15 = (s32[]{:T(128)}, f32[4,768]{1,0:T(4,128)S(1)}, f32[4,768]{1,0:T(4,128)S(1)}, f32[768,4,64]{0,2,1:T(8,128)S(1)}, s32[16]{0:T(128)S(1)}, /*index=5*/s3...) while((s32[]{:T(128)}, f32[4,768]{1,0:T(4,128)S(1)}, ...), condition=%wide.region_5.6_spmd.clone, body=%wide.region_0.5_spmd.clone.sunk | while | flops 649800192 | bytes 33738040 | solution.py:117
  185.8 0.6 dynamic_slice.50
  187.1 13.1 %conditional.3 = ((f32[4,768]{1,0:T(4,128)S(1)}, f32[4,768]{1,0:T(4,128)S(1)}, f32[768,4,64]{0,2,1:T(8,128)S(1)})) conditional(s32[]{:T(128)} %convert_element_type.100, (f32[4,768]{1,0:T(4,128)S(1)}, f32[4,768]{1,0:T(4,128)S(1)}, f32[768,4,64]{0,2,1:T(8,128)S(1)}) %tuple.41, (s32[]{:T(128)}, s32[]{:T(128)}, bf16[16,768,4,64]{1,3,2,0:T(8,128)(2,1)}, ...), branch_computations={%region_1.1_spmd, %region_2.4_spmd} | conditional | flops 649800192 | bytes 33734700 | solution.py:115
  187.1 0.7 iota_add_fusion
  187.7 0.4 broadcast_compare_fusion
  188.2 3.9 fusion.4
  192.0 4.6 fusion.11
  196.6 3.5 fusion.3
  200.2 0.6 dynamic_slice.50
  201.4 0.6 dynamic_slice.50
  202.7 0.6 dynamic_slice.50
  204.0 0.6 dynamic_slice.50
  205.3 0.6 dynamic_slice.50
  206.5 0.6 dynamic_slice.50
  207.8 0.6 dynamic_slice.50
  209.1 0.6 dynamic_slice.50
  210.4 0.6 dynamic_slice.50
  211.7 0.6 dynamic_slice.50
  212.9 0.6 dynamic_slice.50
  214.2 0.6 dynamic_slice.50
  215.5 0.6 dynamic_slice.50
  216.8 0.6 dynamic_slice.50
  218.0 0.6 dynamic_slice.50
  219.3 0.1 divide_convert_fusion
  219.4 0.0 copy-done
  219.4 2.7 convolution_convert_fusion.1
  222.1 4.6 all-to-all-start.1
  226.7 0.2 all-gather.7.cloned.1.call-start
  226.9 38.2 %all-to-all-done.1 = bf16[8,96,2048]{2,1,0:T(8,128)(2,1)} async-done(((bf16[8,96,2048]{2,1,0:T(8,128)(2,1)}), bf16[8,96,2048]{2,1,0:T(8,128)(2,1)}, u32[]{:S(2)}, u32[]{:S(2)}) %all-to-all-start.1) | async-done | bytes 3145760 | tf_op jit(solution)/shard_map/all_to_all | solution.py:41
  265.1 2.5 reduce_sum.59
  267.6 1.2 fusion.33
  268.8 1.3 multiply_reduce_fusion.1
  270.2 2.0 add_convert_fusion.1
  272.2 0.0 all-gather.7.cloned.1.call-update
  272.2 0.0 all-gather.11.cloned.1.call-start
  272.2 0.5 all-gather.11.cloned.1.call-update
  272.8 0.0 reduce-scatter.2.cloned.1.call-start
  272.8 0.0 all-gather.9.cloned.1.call-done
  272.8 220.0 %all-gather.7.cloned.1.call-done = bf16[768,2048]{1,0:T(8,128)(2,1)} async-done(((bf16[96,2048]{1,0:T(8,128)(2,1)}), bf16[768,2048]{1,0:T(8,128)(2,1)}) %all-gather.7.cloned.1.call-update) | async-done | bytes 3145744 | tf_op jit(solution)/shard_map/all_gather | solution.py:153
  492.8 6.5 %fusion.27 = f32[768,704]{0,1:T(8,128)} fusion(bf16[768,2048]{1,0:T(8,128)(2,1)} %all-gather.7.cloned.1.call-done, bf16[2048,1408]{0,1:T(8,128)(2,1)} %all-gather.9.cloned.1.call-done), kind=kOutput, calls=%fused_computation.31 | convolution fusion | flops 2214592512 | bytes 8192000 | tf_op jit(solution)/shard_map/dot_general | solution.py:155
  499.3 46.2 %all-gather.11.cloned.1.call-done = bf16[704,2048]{1,0:T(8,128)(2,1)} async-done(((bf16[704,128]{1,0:T(8,128)(2,1)}), bf16[704,2048]{1,0:T(8,128)(2,1)}) %all-gather.11.cloned.1.call-update) | async-done | bytes 2883600 | tf_op jit(solution)/shard_map/all_gather | solution.py:160
  545.5 12.4 %convolution_convert_fusion = bf16[768,2048]{1,0:T(8,128)(2,1)} fusion(bf16[704,2048]{1,0:T(8,128)(2,1)} %all-gather.11.cloned.1.call-done, f32[768,704]{0,1:T(8,128)} %fusion.27, bf16[768,2048]{1,0:T(8,128)(2,1)} %all-gather.7.cloned.1.call-done, bf16[2048,1408]{0,1:T(8,128)(2,1)} %all-gather.9.cloned.1.call-done), kind=kOutput, calls=%fused_computation.27 | convolution fusion | flops 4434001920 | bytes 14221312 | tf_op jit(solution)/shard_map/dot_general | solution.py:158
  557.9 0.0 reduce-scatter.2.cloned.1.call-update
  557.9 35.3 %reduce-scatter.2.cloned.1.call-done = bf16[96,2048]{1,0:T(8,128)(2,1)} async-done(((bf16[768,2048]{1,0:T(8,128)(2,1)}), bf16[96,2048]{1,0:T(8,128)(2,1)}) %reduce-scatter.2.cloned.1.call-update) | async-done | bytes 393232 | tf_op jit(solution)/shard_map/reduce_scatter | solution.py:163
  593.2 0.0 copy-done.1
  593.2 1.2 fusion.34
  594.4 1.3 multiply_reduce_fusion
  595.7 2.0 add_convert_fusion
  (55 shorter events, 0.3 us)
Async XLA Ops:
  6.5 212.9 %copy-start = (bf16[256,2048]{1,0:T(8,128)(2,1)S(1)}, bf16[256,2048]{1,0:T(8,128)(2,1)}, u32[]{:S(2)}) copy-start(bf16[256,2048]{1,0:T(8,128)(2,1)} %param.22) | copy-start | bytes 3145732
  6.5 95.4 %all-gather.5.cloned.1.call-start = ((), (), s32[]{:S(2)}) async-start(), calls=%async_computation.3 | async-start | bytes 13369344 | tf_op jit(solution)/shard_map/all_gather | solution.py:31
  8.8 264.1 %all-gather.9.cloned.1.call-start = ((), (), s32[]{:S(2)}) async-start(), calls=%async_computation.5 | async-start | bytes 6127616 | tf_op jit(solution)/shard_map/all_gather | solution.py:31
  12.0 173.7 %all-to-all-start = ((f32[16,768,4]{1,2,0:T(4,128)}), f32[16,768,4]{1,2,0:T(4,128)S(1)}, u32[]{:S(2)}, u32[]{:S(2)}) async-start(f32[16,768,4]{1,2,0:T(4,128)} %broadcast_in_dim.56), calls=%async_computation | async-start | bytes 393216 | tf_op jit(solution)/shard_map/all_to_all | solution.py:18
  167.6 18.2 %copy-start.2 = (f32[768,4]{0,1:T(4,128)S(1)}, f32[768,4]{0,1:T(4,128)}, u32[]{:S(2)}) copy-start(f32[768,4]{0,1:T(4,128)} %param.20) | copy-start | bytes 36868
  222.1 48.0 %copy-start.3 = (f32[2048]{0:T(1024)S(1)}, f32[2048]{0:T(1024)}, u32[]{:S(2)}) copy-start(f32[2048]{0:T(1024)} %param.24) | copy-start | bytes 24580
  222.1 48.0 %copy-start.4 = (f32[2048]{0:T(1024)S(1)}, f32[2048]{0:T(1024)}, u32[]{:S(2)}) copy-start(f32[2048]{0:T(1024)} %param.23) | copy-start | bytes 24580
  222.1 43.0 %all-to-all-start.1 = ((bf16[8,96,2048]{2,1,0:T(8,128)(2,1)}), bf16[8,96,2048]{2,1,0:T(8,128)(2,1)}, u32[]{:S(2)}, u32[]{:S(2)}) async-start(bf16[8,96,2048]{2,1,0:T(8,128)(2,1)} %bitcast.45), calls=%async_computation.1 | async-start | bytes 6291456 | tf_op jit(solution)/shard_map/all_to_all | solution.py:41
  226.7 266.1 %all-gather.7.cloned.1.call-start = ((), (), s32[]{:S(2)}) async-start(), calls=%async_computation.4 | async-start | bytes 3538944 | tf_op jit(solution)/shard_map/all_gather | solution.py:153
  272.2 273.3 %all-gather.11.cloned.1.call-start = ((), (), s32[]{:S(2)}) async-start(), calls=%async_computation.6 | async-start | bytes 3063808 | tf_op jit(solution)/shard_map/all_gather | solution.py:160
  272.8 320.4 %reduce-scatter.2.cloned.1.call-start = ((), (), s32[]{:S(2)}) async-start(), calls=%async_computation.7 | async-start | bytes 3538944 | tf_op jit(solution)/shard_map/reduce_scatter | solution.py:163
  499.3 93.9 %copy-start.1 = (bf16[96,2048]{1,0:T(8,128)(2,1)S(1)}, bf16[96,2048]{1,0:T(8,128)(2,1)}, u32[]{:S(2)}) copy-start(bf16[96,2048]{1,0:T(8,128)(2,1)} %add_convert_fusion.1) | copy-start | bytes 1179652
  499.3 96.4 %copy-start.5 = (f32[2048]{0:T(1024)S(1)}, f32[2048]{0:T(1024)}, u32[]{:S(2)}) copy-start(f32[2048]{0:T(1024)} %param.29) | copy-start | bytes 24580
  499.3 96.4 %copy-start.6 = (f32[2048]{0:T(1024)S(1)}, f32[2048]{0:T(1024)}, u32[]{:S(2)}) copy-start(f32[2048]{0:T(1024)} %param.28) | copy-start | bytes 24580
Sparse Core Ops, SparseCore 0:
  9.5 92.3 all-gather.4
  104.0 64.0 all-gather.8
  272.3 220.4 all-gather.6
  494.8 50.6 all-gather.10
  558.0 35.0 reduce-scatter.1
where the time goes:
time: 608 us; the launch traced here: 604 us
  waiting for transfers between devices  421 us (69%)
  local copies, waits for them, and re-layouts  95.9 us (16%)
  matrix products  30.1 us (5%)
  other arithmetic  20.1 us (3%)
  between operations  13.3 us (2%)
  starting transfers between devices  13.1 us (2%)
  loops' own time  11.1 us (2%)
    all_gather x1, waiting for transfers between devices, body(): gathered = lax.all_gather(normed, 'tp', axis=0, tiled=True)  220 us
    all_gather x2, waiting for transfers between devices, in_one_piece(): lax.all_gather(both, axis, axis=dim, tiled=True)  80.5 us
    all_gather x1, waiting for transfers between devices, body(): lax.all_gather(down_weight, 'sp', axis=1, tiled=True)  46.2 us
    all_to_all x1, waiting for transfers between devices, sum_at_owner(): lax.all_to_all(pieces, axis, split_axis=0, concat_axis=0, tiled=True)  38.2 us
    unnamed x17, local copies, waits for them, and re-layouts  37.4 us
    reduce_scatter x1, waiting for transfers between devices, body(): lax.psum_scatter(partial_terms.astype(jnp.bfloat16), 'tp', scatter_dimens...  35.3 us
    reshape x1, local copies, waits for them, and re-layouts, attend(): key_blocks = key_piece.reshape(blocks, block_len, head_count, head_dim)  18.8 us
    reshape x1, local copies, waits for them, and re-layouts, attend(): value_blocks = value_piece.reshape(blocks, block_len, head_count, head_dim)  18.8 us
  transfers between devices with their start and end apart: 7, of which 5 were waited for; matrix products, arithmetic and copies ran while one was open for 21% of the time, Pallas kernels for 0%

commit v1 on v0

--- a/solution.py
+++ b/solution.py
@@ -5,6 +5,11 @@
 
 ALPHA = 8.0**0.25
 EPSILON = 1e-05
+
+
+def gather_by_exchange(x, axis, dim):
+    copies = jnp.concatenate([x] * lax.axis_size(axis), axis=dim)
+    return lax.all_to_all(copies, axis, dim, dim, tiled=True)
 
 
 def laid_out(pieces, dim):
@@ -150,7 +155,7 @@
     normed = layer_norm(
         ALPHA * stream_own.astype(jnp.float32) + mix_out, mix_gain, mix_bias
     ).astype(jnp.bfloat16)
-    gathered = lax.all_gather(normed, "tp", axis=0, tiled=True)
+    gathered = gather_by_exchange(normed, "tp", 0)
     pieces = in_one_piece((gate_weight, up_weight), "sp", 0, 1)
     gate_part = jnp.dot(gathered, pieces[0], preferred_element_type=jnp.float32)
     up_part = jnp.dot(gathered, pieces[1], preferred_element_type=jnp.float32)

time: 608 us -> 579 us (0.952)
  waiting for transfers between devices: 421 us -> 387 us
    all_gather x1 -> x0, waiting for transfers between devices: 220 us -> none  [body(): gathered = lax.all_gather(normed, 'tp', axis=0, tiled=True)]
    all_gather x1, waiting for transfers between devices: 46.2 us -> 153 us  [body(): lax.all_gather(down_weight, 'sp', axis=1, tiled=True)]
    reduce_scatter x1, waiting for transfers between devices: 35.3 us -> 76.1 us  [body(): lax.psum_scatter(partial_terms.astype(jnp.bfloat16), 'tp', scatter_dimens...]
    all_to_all x0 -> x1, waiting for transfers between devices: none -> 38.3 us  [gather_by_exchange(): return lax.all_to_all(copies, axis, dim, dim, tiled=True)]
    unnamed x17 -> x25, local copies, waits for them, and re-layouts: 37.4 us -> 38.2 us
  transfers between devices with their start and end apart: 7 -> 7, of which waited for: 5 -> 5; matrix products, arithmetic and copies ran while one was open for 21% -> 22% of each run, Pallas kernels for 0% -> 0%
where the time goes in v1:
time: 579 us; the launch traced here: 575 us
  waiting for transfers between devices  387 us (67%)
  local copies, waits for them, and re-layouts  96.5 us (17%)
  matrix products  30.1 us (5%)
  other arithmetic  19.3 us (3%)
  starting transfers between devices  17.4 us (3%)
  between operations  13.4 us (2%)
  loops' own time  10.9 us (2%)
    all_gather x1, waiting for transfers between devices, body(): lax.all_gather(down_weight, 'sp', axis=1, tiled=True)  153 us
    all_gather x2, waiting for transfers between devices, in_one_piece(): lax.all_gather(both, axis, axis=dim, tiled=True)  82.2 us
    reduce_scatter x1, waiting for transfers between devices, body(): lax.psum_scatter(partial_terms.astype(jnp.bfloat16), 'tp', scatter_dimens...  76.1 us
    all_to_all x1, waiting for transfers between devices, gather_by_exchange(): return lax.all_to_all(copies, axis, dim, dim, tiled=True)  38.3 us
    unnamed x25, local copies, waits for them, and re-layouts  38.2 us
    all_to_all x1, waiting for transfers between devices, sum_at_owner(): lax.all_to_all(pieces, axis, split_axis=0, concat_axis=0, tiled=True)  37.6 us
    reshape x1, local copies, waits for them, and re-layouts, attend(): key_blocks = key_piece.reshape(blocks, block_len, head_count, head_dim)  18.8 us
    reshape x1, local copies, waits for them, and re-layouts, attend(): value_blocks = value_piece.reshape(blocks, block_len, head_count, head_dim)  18.8 us
  transfers between devices with their start and end apart: 7, of which 5 were waited for; matrix products, arithmetic and copies ran while one was open for 22% of the time, Pallas kernels for 0%

profile of v1, /device:TPU:0, one launch (start us, length us, event | category | flops | bytes accessed | tf_op | source)
XLA Modules:
  0.0 574.9 jit_solution(18210850682517216798)
XLA Ops:
  6.5 2.2 pad_maximum_fusion
  8.8 0.0 all-gather.4.cloned.1.call-update
  8.8 0.0 all-gather.6.cloned.1.call-start
  8.8 1.8 pad_maximum_fusion.1
  10.6 0.0 all-gather.6.cloned.1.call-update
  10.6 0.7 broadcast_in_dim.56
  11.3 8.2 %all-to-all-start = ((f32[16,768,4]{1,2,0:T(4,128)}), f32[16,768,4]{1,2,0:T(4,128)S(1)}, u32[]{:S(2)}, u32[]{:S(2)}) async-start(f32[16,768,4]{1,2,0:T(4,128)} %broadcast_in_dim.56), calls=%async_computation | async-start | bytes 393216 | tf_op jit(solution)/shard_map/all_to_all | solution.py:23
  19.5 0.2 copy.18
  19.7 82.2 %all-gather.4.cloned.1.call-done = bf16[12288,512]{1,0:T(8,128)(2,1)} async-done(((bf16[768,512]{1,0:T(8,128)(2,1)}), bf16[12288,512]{1,0:T(8,128)(2,1)}) %all-gather.4.cloned.1.call-update) | async-done | bytes 12582928 | tf_op jit(solution)/shard_map/all_gather | solution.py:36
  101.9 10.1 %fusion.36 = (bf16[12288,256]{1,0:T(8,128)(2,1)}, bf16[12288,256]{1,0:T(8,128)(2,1)}) fusion(bf16[12288,512]{1,0:T(8,128)(2,1)} %all-gather.4.cloned.1.call-done), kind=kLoop, calls=%fused_computation.59 | loop fusion | bytes 25165824 | tf_op jit(solution)/shard_map/split | solution.py:36
  112.0 18.8 %reshape.84 = bf16[16,768,4,64]{3,2,1,0:T(4,128)(2,1)} reshape(bf16[12288,256]{1,0:T(8,128)(2,1)} %get-tuple-element.251) | data formatting | bytes 12582912 | tf_op jit(solution)/shard_map/reshape | solution.py:85
  130.8 18.1 %copy.20 = bf16[16,768,4,64]{1,3,2,0:T(8,128)(2,1)} copy(bf16[16,768,4,64]{3,2,1,0:T(4,128)(2,1)} %reshape.84) | data formatting | bytes 12582912
  148.9 18.8 %reshape.85 = bf16[16,768,4,64]{3,2,1,0:T(4,128)(2,1)} reshape(bf16[12288,256]{1,0:T(8,128)(2,1)} %get-tuple-element.250) | data formatting | bytes 12582912 | tf_op jit(solution)/shard_map/reshape | solution.py:86
  167.6 18.1 %copy.21 = bf16[16,768,4,64]{1,3,2,0:T(8,128)(2,1)} copy(bf16[16,768,4,64]{3,2,1,0:T(4,128)(2,1)} %reshape.85) | data formatting | bytes 12582912
  185.7 0.0 all-to-all-done
  185.7 0.1 broadcast_in_dim.55
  185.8 33.7 %while.15 = (s32[]{:T(128)}, f32[4,768]{1,0:T(4,128)S(1)}, f32[4,768]{1,0:T(4,128)S(1)}, f32[768,4,64]{0,2,1:T(8,128)S(1)}, s32[16]{0:T(128)S(1)}, /*index=5*/s3...) while((s32[]{:T(128)}, f32[4,768]{1,0:T(4,128)S(1)}, ...), condition=%wide.region_5.6_spmd.clone, body=%wide.region_0.5_spmd.clone.sunk | while | flops 649800192 | bytes 33738040 | solution.py:122
  185.8 0.6 dynamic_slice.51
  187.1 13.1 %conditional.3 = ((f32[4,768]{1,0:T(4,128)S(1)}, f32[4,768]{1,0:T(4,128)S(1)}, f32[768,4,64]{0,2,1:T(8,128)S(1)})) conditional(s32[]{:T(128)} %convert_element_type.103, (f32[4,768]{1,0:T(4,128)S(1)}, f32[4,768]{1,0:T(4,128)S(1)}, f32[768,4,64]{0,2,1:T(8,128)S(1)}) %tuple.42, (s32[]{:T(128)}, s32[]{:T(128)}, bf16[16,768,4,64]{1,3,2,0:T(8,128)(2,1)}, ...), branch_computations={%region_1.1_spmd, %region_2.4_spmd} | conditional | flops 649800192 | bytes 33734700 | solution.py:120
  187.1 0.6 iota_add_fusion
  187.7 0.4 broadcast_compare_fusion
  188.1 3.9 fusion.4
  192.0 4.6 fusion.11
  196.6 3.5 fusion.3
  200.1 0.6 dynamic_slice.51
  201.4 0.6 dynamic_slice.51
  202.7 0.6 dynamic_slice.51
  204.0 0.6 dynamic_slice.51
  205.3 0.6 dynamic_slice.51
  206.6 0.6 dynamic_slice.51
  207.9 0.6 dynamic_slice.51
  209.2 0.6 dynamic_slice.51
  210.5 0.6 dynamic_slice.51
  211.8 0.6 dynamic_slice.51
  213.1 0.6 dynamic_slice.51
  214.3 0.6 dynamic_slice.51
  215.6 0.6 dynamic_slice.51
  216.9 0.6 dynamic_slice.51
  218.2 0.6 dynamic_slice.51
  219.5 0.1 divide_convert_fusion
  219.6 2.7 convolution_convert_fusion.1
  222.3 4.4 all-to-all-start.1
  226.7 0.0 copy-start.4
  226.8 0.0 copy-start.5
  226.8 0.2 all-gather.8.cloned.1.call-start
  227.0 0.5 all-gather.8.cloned.1.call-update
  227.5 37.6 %all-to-all-done.1 = bf16[8,96,2048]{2,1,0:T(8,128)(2,1)} async-done(((bf16[8,96,2048]{2,1,0:T(8,128)(2,1)}), bf16[8,96,2048]{2,1,0:T(8,128)(2,1)}, u32[]{:S(2)}, u32[]{:S(2)}) %all-to-all-start.1) | async-done | bytes 3145760 | tf_op jit(solution)/shard_map/all_to_all | solution.py:46
  265.2 2.5 reduce_sum.59
  267.6 1.2 fusion.33
  268.9 1.3 multiply_reduce_fusion.1
  270.2 1.2 constant_dynamic-update-slice_fusion.7
  271.7 1.7 copy-done.1
  273.4 4.4 all-to-all-start.2
  277.8 0.0 reduce-scatter.2.cloned.1.call-start
  277.9 0.0 all-gather.6.cloned.1.call-done
  277.9 38.3 %all-to-all-done.2 = bf16[8,96,2048]{2,1,0:T(8,128)(2,1)} async-done(((bf16[8,96,2048]{2,1,0:T(8,128)(2,1)}), bf16[8,96,2048]{2,1,0:T(8,128)(2,1)}, u32[]{:S(2)}, u32[]{:S(2)}) %all-to-all-start.2) | async-done | bytes 3145760 | tf_op jit(solution)/shard_map/all_to_all | solution.py:12
  316.2 6.5 %fusion.27 = f32[768,704]{0,1:T(8,128)} fusion(bf16[768,2048]{1,0:T(8,128)(2,1)} %bitcast.13, bf16[2048,1408]{0,1:T(8,128)(2,1)} %all-gather.6.cloned.1.call-done), kind=kOutput, calls=%fused_computation.31 | convolution fusion | flops 2214592512 | bytes 8192000 | tf_op jit(solution)/shard_map/dot_general | solution.py:160
  322.8 152.5 %all-gather.8.cloned.1.call-done = bf16[704,2048]{1,0:T(8,128)(2,1)} async-done(((bf16[704,128]{1,0:T(8,128)(2,1)}), bf16[704,2048]{1,0:T(8,128)(2,1)}) %all-gather.8.cloned.1.call-update) | async-done | bytes 2883600 | tf_op jit(solution)/shard_map/all_gather | solution.py:165
  475.3 12.4 %convolution_convert_fusion = bf16[768,2048]{1,0:T(8,128)(2,1)} fusion(bf16[704,2048]{1,0:T(8,128)(2,1)} %all-gather.8.cloned.1.call-done, f32[768,704]{0,1:T(8,128)} %fusion.27, bf16[768,2048]{1,0:T(8,128)(2,1)} %bitcast.13, bf16[2048,1408]{0,1:T(8,128)(2,1)} %all-gather.6.cloned.1.call-done), kind=kOutput, calls=%fused_computation.27 | convolution fusion | flops 4434001920 | bytes 14221312 | tf_op jit(solution)/shard_map/dot_general | solution.py:163
  487.7 0.0 reduce-scatter.2.cloned.1.call-update
  487.7 76.1 %reduce-scatter.2.cloned.1.call-done = bf16[96,2048]{1,0:T(8,128)(2,1)} async-done(((bf16[768,2048]{1,0:T(8,128)(2,1)}), bf16[96,2048]{1,0:T(8,128)(2,1)}) %reduce-scatter.2.cloned.1.call-update) | async-done | bytes 393232 | tf_op jit(solution)/shard_map/reduce_scatter | solution.py:168
  563.9 1.2 fusion.34
  565.1 1.3 multiply_reduce_fusion
  566.4 2.0 add_convert_fusion
  (63 shorter events, 0.5 us)
Async XLA Ops:
  6.5 213.0 %copy-start = (bf16[256,2048]{1,0:T(8,128)(2,1)S(1)}, bf16[256,2048]{1,0:T(8,128)(2,1)}, u32[]{:S(2)}) copy-start(bf16[256,2048]{1,0:T(8,128)(2,1)} %param.22) | copy-start | bytes 3145732
  6.5 4.1 copy-start.2
  6.5 13.0 %copy-start.3 = (bf16[768,256]{1,0:T(8,128)(2,1)S(1)}, bf16[768,256]{1,0:T(8,128)(2,1)}, u32[]{:S(2)}) copy-start(bf16[768,256]{1,0:T(8,128)(2,1)} %param.17) | copy-start | bytes 1179652
  6.5 95.4 %all-gather.4.cloned.1.call-start = ((), (), s32[]{:S(2)}) async-start(), calls=%async_computation.4 | async-start | bytes 13369344 | tf_op jit(solution)/shard_map/all_gather | solution.py:36
  8.8 269.1 %all-gather.6.cloned.1.call-start = ((), (), s32[]{:S(2)}) async-start(), calls=%async_computation.5 | async-start | bytes 6127616 | tf_op jit(solution)/shard_map/all_gather | solution.py:36
  11.3 174.4 %all-to-all-start = ((f32[16,768,4]{1,2,0:T(4,128)}), f32[16,768,4]{1,2,0:T(4,128)S(1)}, u32[]{:S(2)}, u32[]{:S(2)}) async-start(f32[16,768,4]{1,2,0:T(4,128)} %broadcast_in_dim.56), calls=%async_computation | async-start | bytes 393216 | tf_op jit(solution)/shard_map/all_to_all | solution.py:23
  222.3 42.9 %all-to-all-start.1 = ((bf16[8,96,2048]{2,1,0:T(8,128)(2,1)}), bf16[8,96,2048]{2,1,0:T(8,128)(2,1)}, u32[]{:S(2)}, u32[]{:S(2)}) async-start(bf16[8,96,2048]{2,1,0:T(8,128)(2,1)} %bitcast.47), calls=%async_computation.1 | async-start | bytes 6291456 | tf_op jit(solution)/shard_map/all_to_all | solution.py:46
  226.7 43.4 %copy-start.4 = (f32[2048]{0:T(1024)S(1)}, f32[2048]{0:T(1024)}, u32[]{:S(2)}) copy-start(f32[2048]{0:T(1024)} %param.24) | copy-start | bytes 24580
  226.8 43.4 %copy-start.5 = (f32[2048]{0:T(1024)S(1)}, f32[2048]{0:T(1024)}, u32[]{:S(2)}) copy-start(f32[2048]{0:T(1024)} %param.23) | copy-start | bytes 24580
  226.8 248.5 %all-gather.8.cloned.1.call-start = ((), (), s32[]{:S(2)}) async-start(), calls=%async_computation.6 | async-start | bytes 3063808 | tf_op jit(solution)/shard_map/all_gather | solution.py:165
  271.7 1.7 copy-start.1
  273.4 42.9 %all-to-all-start.2 = ((bf16[8,96,2048]{2,1,0:T(8,128)(2,1)}), bf16[8,96,2048]{2,1,0:T(8,128)(2,1)}, u32[]{:S(2)}, u32[]{:S(2)}) async-start(bf16[8,96,2048]{2,1,0:T(8,128)(2,1)} %bitcast.48), calls=%async_computation.2 | async-start | bytes 6291456 | tf_op jit(solution)/shard_map/all_to_all | solution.py:12
  277.8 286.0 %reduce-scatter.2.cloned.1.call-start = ((), (), s32[]{:S(2)}) async-start(), calls=%async_computation.7 | async-start | bytes 3538944 | tf_op jit(solution)/shard_map/reduce_scatter | solution.py:168
  487.7 78.7 %copy-start.6 = (f32[2048]{0:T(1024)S(1)}, f32[2048]{0:T(1024)}, u32[]{:S(2)}) copy-start(f32[2048]{0:T(1024)} %param.29) | copy-start | bytes 24580
  487.7 78.7 %copy-start.7 = (f32[2048]{0:T(1024)S(1)}, f32[2048]{0:T(1024)}, u32[]{:S(2)}) copy-start(f32[2048]{0:T(1024)} %param.28) | copy-start | bytes 24580
Sparse Core Ops, SparseCore 0:
  9.5 92.3 all-gather.3
  104.0 64.0 all-gather.5
  229.7 245.5 all-gather.7
  487.9 75.9 reduce-scatter.1
